TPU v7x, 32 devices: a whole 2x2x4 slice. The times are simulated.
32 devices in a mesh: fs: 4 (over y, x), tp: 8 (over z, core).
Axes of the slice: x: 2, y: 2, z: 4, core: 2. Of those that a mesh axis runs over, the one named last changes fastest.
Arguments:
- tokens: bfloat16 [4096, 2048], P(('fs', 'tp')), may hold values from -6 to 6
- norm_gain: float32 [2048], replicated, may hold values from 0.1 to 1.9
- gate_weight: bfloat16 [2048, 5632], P('fs', 'tp'), may hold values from -0.125 to 0.125
- up_weight: bfloat16 [2048, 5632], P('fs', 'tp'), may hold values from -0.125 to 0.125
- down_weight: bfloat16 [5632, 2048], P('tp', 'fs'), may hold values from -0.078125 to 0.078125
Outputs:
- mixed: bfloat16 [4096, 2048], P(('fs', 'tp'))
All inputs are finite; a program needn't handle non-finite values.
Results may differ from a plain program's by a relative error of at most 0.0065.
Values may be sent and summed in bfloat16 or wider, within the bound.
A program may use at most 128 MiB of HBM per device.

v0:
```python
import jax
import jax.numpy as jnp
from jax import lax
from jax.sharding import PartitionSpec as P

eps_floor = 0.05


def local(tokens, norm_gain, gate_weight, up_weight, down_weight):
    values = tokens.astype(jnp.float32)
    factor = lax.rsqrt(jnp.mean(values * values, axis=-1, keepdims=True) + eps_floor)
    normed = (values * factor * norm_gain).astype(jnp.bfloat16)
    local_ff = gate_weight.shape[1]
    group = lax.all_gather(normed, "tp", axis=0, tiled=True)
    joined = jnp.concatenate(
        (
            lax.all_gather(gate_weight, "fs", axis=0, tiled=True),
            lax.all_gather(up_weight, "fs", axis=0, tiled=True),
        ),
        axis=1,
    )
    product = jnp.dot(group, joined, preferred_element_type=jnp.float32)
    hidden = (jax.nn.silu(product[:, :local_ff]) * product[:, local_ff:]).astype(jnp.bfloat16)
    down_local = lax.all_gather(down_weight, "fs", axis=1, tiled=True)
    mixed = lax.psum_scatter(
        jnp.dot(hidden, down_local, preferred_element_type=jnp.float32),
        "tp",
        scatter_dimension=0,
        tiled=True,
    )
    return mixed.astype(jnp.bfloat16)


def solution(mesh):
    return jax.shard_map(
        local,
        mesh=mesh,
        in_specs=(P(("fs", "tp"), None), P(), P("fs", "tp"), P("fs", "tp"), P("tp", "fs")),
        out_specs=P(("fs", "tp"), None),
        check_vma=False,
    )
```

profile of v0, /device:TPU:0, one launch (start us, length us, event | category | flops | bytes accessed | tf_op | source)
XLA Modules:
  0.0 296.1 jit_solution(4076748041551358290)
XLA Ops:
  6.5 0.0 all-gather.7.cloned.1.call-start
  6.5 0.7 all-gather.7.cloned.1.call-update
  7.3 0.0 all-gather.9.cloned.1.call-start
  7.3 0.7 all-gather.9.cloned.1.call-update
  8.0 0.0 all-gather.5.cloned.1.call-start
  8.1 1.2 fusion.8
  9.3 2.0 fusion.10
  11.3 0.0 all-gather.5.cloned.1.call-update
  11.3 0.0 all-gather.11.cloned.1.call-start
  11.4 0.5 all-gather.11.cloned.1.call-update
  11.9 0.0 reduce-scatter.2.cloned.1.call-start
  12.0 41.5 %all-gather.7.cloned.1.call-done = bf16[2048,704]{0,1:T(8,128)(2,1)} async-done(((bf16[512,704]{0,1:T(8,128)(2,1)}), bf16[2048,704]{0,1:T(8,128)(2,1)}) %all-gather.7.cloned.1.call-update) | async-done | bytes 2883600 | tf_op jit(solution)/shard_map/all_gather | solution.py:17
  53.5 43.4 %all-gather.9.cloned.1.call-done = bf16[2048,704]{0,1:T(8,128)(2,1)} async-done(((bf16[512,704]{0,1:T(8,128)(2,1)}), bf16[2048,704]{0,1:T(8,128)(2,1)}) %all-gather.9.cloned.1.call-update) | async-done | bytes 2883600 | tf_op jit(solution)/shard_map/all_gather | solution.py:18
  96.9 48.5 %all-gather.5.cloned.1.call-done = bf16[1024,2048]{1,0:T(8,128)(2,1)} async-done(((bf16[128,2048]{1,0:T(8,128)(2,1)}), bf16[1024,2048]{1,0:T(8,128)(2,1)}) %all-gather.5.cloned.1.call-update) | async-done | bytes 4194320 | tf_op jit(solution)/shard_map/all_gather | solution.py:14
  145.4 11.8 %fusion = f32[1024,1408]{1,0:T(8,128)} fusion(bf16[1024,2048]{1,0:T(8,128)(2,1)} %all-gather.5.cloned.1.call-done, bf16[2048,704]{0,1:T(8,128)(2,1)} %all-gather.9.cloned.1.call-done, bf16[2048,704]{0,1:T(8,128)(2,1)} %all-gather.7.cloned.1.call-done), kind=kOutput, calls=%fused_computation | convolution fusion | flops 5917114368 | bytes 15728640 | tf_op jit(solution)/shard_map/dot_general | solution.py:22
  157.2 30.2 %all-gather.11.cloned.1.call-done = bf16[704,2048]{1,0:T(8,128)(2,1)} async-done(((bf16[704,512]{1,0:T(8,128)(2,1)}), bf16[704,2048]{1,0:T(8,128)(2,1)}) %all-gather.11.cloned.1.call-update) | async-done | bytes 2883600 | tf_op jit(solution)/shard_map/all_gather | solution.py:24
  187.4 10.4 %fusion.5 = f32[1024,2048]{1,0:T(8,128)} fusion(bf16[704,2048]{1,0:T(8,128)(2,1)} %all-gather.11.cloned.1.call-done, f32[1024,1408]{1,0:T(8,128)} %fusion), kind=kOutput, calls=%fused_computation.6 | convolution fusion | flops 2957115392 | bytes 17563648 | tf_op jit(solution)/shard_map/dot_general | solution.py:26
  197.8 0.0 reduce-scatter.2.cloned.1.call-update
  197.8 89.7 %reduce-scatter.2.cloned.1.call-done = f32[128,2048]{1,0:T(8,128)} async-done(((f32[1024,2048]{1,0:T(8,128)}), f32[128,2048]{1,0:T(8,128)}) %reduce-scatter.2.cloned.1.call-update) | async-done | bytes 1048592 | tf_op jit(solution)/shard_map/reduce_scatter | solution.py:25
  287.5 2.1 convert_element_type.15
  (1 shorter events, 0.0 us)
Async XLA Ops:
  6.5 46.9 %all-gather.7.cloned.1.call-start = ((), (), s32[]{:S(2)}) async-start(), calls=%async_computation.2 | async-start | bytes 3604480 | tf_op jit(solution)/shard_map/all_gather | solution.py:17
  7.3 89.6 %all-gather.9.cloned.1.call-start = ((), (), s32[]{:S(2)}) async-start(), calls=%async_computation.3 | async-start | bytes 3604480 | tf_op jit(solution)/shard_map/all_gather | solution.py:18
  8.0 137.3 %all-gather.5.cloned.1.call-start = ((), (), s32[]{:S(2)}) async-start(), calls=%async_computation.1 | async-start | bytes 4718592 | tf_op jit(solution)/shard_map/all_gather | solution.py:14
  11.3 176.1 %all-gather.11.cloned.1.call-start = ((), (), s32[]{:S(2)}) async-start(), calls=%async_computation.4 | async-start | bytes 3604480 | tf_op jit(solution)/shard_map/all_gather | solution.py:24
  11.9 275.6 %reduce-scatter.2.cloned.1.call-start = ((), (), s32[]{:S(2)}) async-start(), calls=%async_computation.5 | async-start | bytes 9437184 | tf_op jit(solution)/shard_map/reduce_scatter | solution.py:25
Sparse Core Ops, SparseCore 0:
  9.2 44.2 all-gather.6
  55.3 41.5 all-gather.8
  98.5 46.8 all-gather.4
  147.0 40.3 all-gather.10
  198.0 89.5 reduce-scatter.1
where the time goes:
time: 296 us
  waiting for transfers between devices  255 us (86%)
  matrix products  22.2 us (8%)
  between operations  13.1 us (4%)
  other arithmetic  5.35 us (2%)
    reduce_scatter x1, waiting for transfers between devices, local(): lax.psum_scatter(jnp.dot(hidden, down_local, preferred_element_type=jnp.f...  89.7 us
    all_gather x1, waiting for transfers between devices, local(): group = lax.all_gather(normed, 'tp', axis=0, tiled=True)  48.5 us
    all_gather x1, waiting for transfers between devices, local(): lax.all_gather(up_weight, 'fs', axis=0, tiled=True)  43.4 us
    all_gather x1, waiting for transfers between devices, local(): lax.all_gather(gate_weight, 'fs', axis=0, tiled=True)  41.5 us
    all_gather x1, waiting for transfers between devices, local(): down_local = lax.all_gather(down_weight, 'fs', axis=1, tiled=True)  30.2 us
    dot_general x1, matrix products, local(): product = jnp.dot(group, joined, preferred_element_type=jnp.float32)  11.8 us
    dot_general x1, matrix products, local(): jnp.dot(hidden, down_local, preferred_element_type=jnp.float32)  10.4 us
  transfers between devices with their start and end apart: 5, of which 5 were waited for; matrix products, arithmetic and copies ran while one was open for 5% of the time, Pallas kernels for 0%

commit v1 on v0

--- a/solution.py
+++ b/solution.py
@@ -11,7 +11,12 @@
     factor = lax.rsqrt(jnp.mean(values * values, axis=-1, keepdims=True) + eps_floor)
     normed = (values * factor * norm_gain).astype(jnp.bfloat16)
     local_ff = gate_weight.shape[1]
-    group = lax.all_gather(normed, "tp", axis=0, tiled=True)
+    ring = [normed]
+    for hop in range(7):
+        ring.append(lax.ppermute(ring[-1], "tp", [(dev, (dev + 1) % 8) for dev in range(8)]))
+    group = jnp.roll(
+        jnp.concatenate(ring[::-1], axis=0), (lax.axis_index("tp") + 1) * ring[0].shape[0], axis=0
+    )
     joined = jnp.concatenate(
         (
             lax.all_gather(gate_weight, "fs", axis=0, tiled=True),

time: 296 us -> 249 us (0.84)
  waiting for transfers between devices: 255 us -> 190 us
  local copies, waits for them, and re-layouts: 0 us -> 16 us
    ppermute x0 -> x7, waiting for transfers between devices: none -> 73.6 us  [local(): lax.ppermute(ring[-1], 'tp', [(dev, (dev + 1) % 8) for dev in range(8)])]
    all_gather x1 -> x0, waiting for transfers between devices: 48.5 us -> none  [local(): group = lax.all_gather(normed, 'tp', axis=0, tiled=True)]
    all_gather x1, waiting for transfers between devices: 43.4 us -> 0.01 us  [local(): lax.all_gather(up_weight, 'fs', axis=0, tiled=True)]
    all_gather x1, waiting for transfers between devices: 41.5 us -> 0.01 us  [local(): lax.all_gather(gate_weight, 'fs', axis=0, tiled=True)]
    unnamed x0 -> x18, local copies, waits for them, and re-layouts: none -> 16 us
    all_gather x1, waiting for transfers between devices: 30.2 us -> 25.2 us  [local(): down_local = lax.all_gather(down_weight, 'fs', axis=1, tiled=True)]
  transfers between devices with their start and end apart: 5 -> 11, of which waited for: 5 -> 9; matrix products, arithmetic and copies ran while one was open for 5% -> 13% of each run, Pallas kernels for 0% -> 0%
where the time goes in v1:
time: 249 us
  waiting for transfers between devices  190 us (76%)
  matrix products  22.6 us (9%)
  local copies, waits for them, and re-layouts  16 us (6%)
  between operations  13.2 us (5%)
  other arithmetic  6.57 us (3%)
    reduce_scatter x1, waiting for transfers between devices, local(): lax.psum_scatter(jnp.dot(hidden, down_local, preferred_element_type=jnp.f...  89.7 us
    ppermute x7, waiting for transfers between devices, local(): lax.ppermute(ring[-1], 'tp', [(dev, (dev + 1) % 8) for dev in range(8)])  73.6 us
    all_gather x1, waiting for transfers between devices, local(): down_local = lax.all_gather(down_weight, 'fs', axis=1, tiled=True)  25.2 us
    unnamed x18, local copies, waits for them, and re-layouts  16 us
    dot_general x1, matrix products, local(): product = jnp.dot(group, joined, preferred_element_type=jnp.float32)  12.2 us
    dot_general x1, matrix products, local(): jnp.dot(hidden, down_local, preferred_element_type=jnp.float32)  10.4 us
  transfers between devices with their start and end apart: 11, of which 9 were waited for; matrix products, arithmetic and copies ran while one was open for 13% of the time, Pallas kernels for 0%

profile of v1, /device:TPU:0, one launch (start us, length us, event | category | flops | bytes accessed | tf_op | source)
XLA Modules:
  0.0 249.0 jit_solution(5441506715298183775)
XLA Ops:
  8.1 1.2 fusion.9
  9.3 1.2 fusion.11
  11.1 10.9 %collective-permute-done = bf16[128,2048]{1,0:T(8,128)(2,1)S(1)} collective-permute-done((bf16[128,2048]{1,0:T(8,128)(2,1)S(1)}, bf16[128,2048]{1,0:T(8,128)(2,1)S(1)}, u32[]{:S(2)}, u32[]{:S(2)}) %collective-permute-start) | collective-permute-done | bytes 524320 | tf_op jit(solution)/shard_map/ppermute | solution.py:16
  22.0 10.4 %collective-permute-done.1 = bf16[128,2048]{1,0:T(8,128)(2,1)S(1)} collective-permute-done((bf16[128,2048]{1,0:T(8,128)(2,1)S(1)}, bf16[128,2048]{1,0:T(8,128)(2,1)S(1)}, u32[]{:S(2)}, u32[]{:S(2)}) %collective-permute-start.1) | collective-permute-done | bytes 524320 | tf_op jit(solution)/shard_map/ppermute | solution.py:16
  32.4 10.4 %collective-permute-done.2 = bf16[128,2048]{1,0:T(8,128)(2,1)S(1)} collective-permute-done((bf16[128,2048]{1,0:T(8,128)(2,1)S(1)}, bf16[128,2048]{1,0:T(8,128)(2,1)S(1)}, u32[]{:S(2)}, u32[]{:S(2)}) %collective-permute-start.2) | collective-permute-done | bytes 524320 | tf_op jit(solution)/shard_map/ppermute | solution.py:16
  42.8 10.4 %collective-permute-done.3 = bf16[128,2048]{1,0:T(8,128)(2,1)S(1)} collective-permute-done((bf16[128,2048]{1,0:T(8,128)(2,1)S(1)}, bf16[128,2048]{1,0:T(8,128)(2,1)S(1)}, u32[]{:S(2)}, u32[]{:S(2)}) %collective-permute-start.3) | collective-permute-done | bytes 524320 | tf_op jit(solution)/shard_map/ppermute | solution.py:16
  53.2 10.4 %collective-permute-done.4 = bf16[128,2048]{1,0:T(8,128)(2,1)S(1)} collective-permute-done((bf16[128,2048]{1,0:T(8,128)(2,1)S(1)}, bf16[128,2048]{1,0:T(8,128)(2,1)S(1)}, u32[]{:S(2)}, u32[]{:S(2)}) %collective-permute-start.4) | collective-permute-done | bytes 524320 | tf_op jit(solution)/shard_map/ppermute | solution.py:16
  63.6 10.5 %collective-permute-done.5 = bf16[128,2048]{1,0:T(8,128)(2,1)} collective-permute-done((bf16[128,2048]{1,0:T(8,128)(2,1)S(1)}, bf16[128,2048]{1,0:T(8,128)(2,1)}, u32[]{:S(2)}, u32[]{:S(2)}) %collective-permute-start.5) | collective-permute-done | bytes 524320 | tf_op jit(solution)/shard_map/ppermute | solution.py:16
  74.2 10.6 %collective-permute-done.6 = bf16[128,2048]{1,0:T(8,128)(2,1)} collective-permute-done((bf16[128,2048]{1,0:T(8,128)(2,1)}, bf16[128,2048]{1,0:T(8,128)(2,1)}, u32[]{:S(2)}, u32[]{:S(2)}) %collective-permute-start.6) | collective-permute-done | bytes 524320 | tf_op jit(solution)/shard_map/ppermute | solution.py:16
  84.8 1.9 constant_dynamic-update-slice_fusion.15
  86.7 1.9 constant_dynamic-update-slice_fusion.14
  88.6 0.9 constant_dynamic-update-slice_fusion.13
  91.1 0.8 constant_dynamic-update-slice_fusion.10
  92.0 0.8 constant_dynamic-update-slice_fusion.9
  92.8 1.0 constant_dynamic-update-slice_fusion.8
  93.8 1.9 constant_dynamic-update-slice_fusion.7
  95.7 1.9 constant_dynamic-update-slice_fusion.6
  97.6 0.9 constant_dynamic-update-slice_fusion.5
  101.8 1.0 constant_dynamic-update-slice_fusion
  102.9 12.2 %fusion = f32[1024,1408]{1,0:T(8,128)} fusion(bf16[2048,704]{0,1:T(8,128)(2,1)} %all-gather.6.cloned.1.call-done, bf16[2048,704]{0,1:T(8,128)(2,1)} %all-gather.4.cloned.1.call-done, bf16[2048,2048]{1,0:T(8,128)(2,1)} %constant_dynamic-update-slice_fusion, s32[]{:T(128)S(6)} %select_n.14), kind=kOutput, calls=%fused_computation | convolution fusion | flops 5917114368 | bytes 15728644 | tf_op jit(solution)/shard_map/dot_general | solution.py:27
  115.0 25.2 %all-gather.8.cloned.1.call-done = bf16[704,2048]{1,0:T(8,128)(2,1)} async-done(((bf16[704,512]{1,0:T(8,128)(2,1)}), bf16[704,2048]{1,0:T(8,128)(2,1)}) %all-gather.8.cloned.1.call-update) | async-done | bytes 2883600 | tf_op jit(solution)/shard_map/all_gather | solution.py:29
  140.3 10.4 %fusion.6 = f32[1024,2048]{1,0:T(8,128)} fusion(bf16[704,2048]{1,0:T(8,128)(2,1)} %all-gather.8.cloned.1.call-done, f32[1024,1408]{1,0:T(8,128)} %fusion), kind=kOutput, calls=%fused_computation.7 | convolution fusion | flops 2957115392 | bytes 17563648 | tf_op jit(solution)/shard_map/dot_general | solution.py:31
  150.7 89.7 %reduce-scatter.2.cloned.1.call-done = f32[128,2048]{1,0:T(8,128)} async-done(((f32[1024,2048]{1,0:T(8,128)}), f32[128,2048]{1,0:T(8,128)}) %reduce-scatter.2.cloned.1.call-update) | async-done | bytes 1048592 | tf_op jit(solution)/shard_map/reduce_scatter | solution.py:30
  240.4 2.1 convert_element_type.15
  (28 shorter events, 7.2 us)
Async XLA Ops:
  6.5 86.3 %copy-start = (bf16[128,2048]{1,0:T(8,128)(2,1)S(1)}, bf16[128,2048]{1,0:T(8,128)(2,1)}, u32[]{:S(2)}) copy-start(bf16[128,2048]{1,0:T(8,128)(2,1)} %param.5) | copy-start | bytes 1572868
  6.5 86.3 %copy-start.1 = (f32[2048]{0:T(1024)S(1)}, f32[2048]{0:T(1024)}, u32[]{:S(2)}) copy-start(f32[2048]{0:T(1024)} %param.6) | copy-start | bytes 24580
  6.5 96.3 %all-gather.4.cloned.1.call-start = ((), (), s32[]{:S(2)}) async-start(), calls=%async_computation.1 | async-start | bytes 3604480 | tf_op jit(solution)/shard_map/all_gather | solution.py:22
  7.3 95.6 %all-gather.6.cloned.1.call-start = ((), (), s32[]{:S(2)}) async-start(), calls=%async_computation.2 | async-start | bytes 3604480 | tf_op jit(solution)/shard_map/all_gather | solution.py:23
  8.0 132.2 %all-gather.8.cloned.1.call-start = ((), (), s32[]{:S(2)}) async-start(), calls=%async_computation.3 | async-start | bytes 3604480 | tf_op jit(solution)/shard_map/all_gather | solution.py:29
  10.5 11.4 %collective-permute-start = (bf16[128,2048]{1,0:T(8,128)(2,1)S(1)}, bf16[128,2048]{1,0:T(8,128)(2,1)S(1)}, u32[]{:S(2)}, u32[]{:S(2)}) collective-permute-start(bf16[128,2048]{1,0:T(8,128)(2,1)S(1)} %fusion.11), channel_id=1, source_target_pairs={{0,1},{1,2},{2,3},{3,4},{4,5},{5,6},{6,7},{7,0},{8,9},{9,10},{10,1... | collective-permute-start | bytes 1572872 | tf_op jit(solution)/shard_map/ppermute | solution.py:16
  22.0 10.4 %collective-permute-start.1 = (bf16[128,2048]{1,0:T(8,128)(2,1)S(1)}, bf16[128,2048]{1,0:T(8,128)(2,1)S(1)}, u32[]{:S(2)}, u32[]{:S(2)}) collective-permute-start(bf16[128,2048]{1,0:T(8,128)(2,1)S(1)} %collective-permute-done), channel_id=1, source_target_pairs={{0,1},{1,2},{2,3},{3,4},{4,5},{5,6},{6,7},{7,0},{8,9},{9,10},{10,1... | collective-permute-start | bytes 1572872 | tf_op jit(solution)/shard_map/ppermute | solution.py:16
  32.4 10.4 %collective-permute-start.2 = (bf16[128,2048]{1,0:T(8,128)(2,1)S(1)}, bf16[128,2048]{1,0:T(8,128)(2,1)S(1)}, u32[]{:S(2)}, u32[]{:S(2)}) collective-permute-start(bf16[128,2048]{1,0:T(8,128)(2,1)S(1)} %collective-permute-done.1), channel_id=1, source_target_pairs={{0,1},{1,2},{2,3},{3,4},{4,5},{5,6},{6,7},{7,0},{8,9},{9,10},{10,1... | collective-permute-start | bytes 1572872 | tf_op jit(solution)/shard_map/ppermute | solution.py:16
  42.8 10.4 %collective-permute-start.3 = (bf16[128,2048]{1,0:T(8,128)(2,1)S(1)}, bf16[128,2048]{1,0:T(8,128)(2,1)S(1)}, u32[]{:S(2)}, u32[]{:S(2)}) collective-permute-start(bf16[128,2048]{1,0:T(8,128)(2,1)S(1)} %collective-permute-done.2), channel_id=1, source_target_pairs={{0,1},{1,2},{2,3},{3,4},{4,5},{5,6},{6,7},{7,0},{8,9},{9,10},{10,1... | collective-permute-start | bytes 1572872 | tf_op jit(solution)/shard_map/ppermute | solution.py:16
  53.2 10.4 %collective-permute-start.4 = (bf16[128,2048]{1,0:T(8,128)(2,1)S(1)}, bf16[128,2048]{1,0:T(8,128)(2,1)S(1)}, u32[]{:S(2)}, u32[]{:S(2)}) collective-permute-start(bf16[128,2048]{1,0:T(8,128)(2,1)S(1)} %collective-permute-done.3), channel_id=1, source_target_pairs={{0,1},{1,2},{2,3},{3,4},{4,5},{5,6},{6,7},{7,0},{8,9},{9,10},{10,1... | collective-permute-start | bytes 1572872 | tf_op jit(solution)/shard_map/ppermute | solution.py:16
  63.6 10.5 %collective-permute-start.5 = (bf16[128,2048]{1,0:T(8,128)(2,1)S(1)}, bf16[128,2048]{1,0:T(8,128)(2,1)}, u32[]{:S(2)}, u32[]{:S(2)}) collective-permute-start(bf16[128,2048]{1,0:T(8,128)(2,1)S(1)} %collective-permute-done.4), channel_id=1, source_target_pairs={{0,1},{1,2},{2,3},{3,4},{4,5},{5,6},{6,7},{7,0},{8,9},{9,10},{10,1... | collective-permute-start | bytes 1572872 | tf_op jit(solution)/shard_map/ppermute | solution.py:16
  74.1 10.7 %collective-permute-start.6 = (bf16[128,2048]{1,0:T(8,128)(2,1)}, bf16[128,2048]{1,0:T(8,128)(2,1)}, u32[]{:S(2)}, u32[]{:S(2)}) collective-permute-start(bf16[128,2048]{1,0:T(8,128)(2,1)} %collective-permute-done.5), channel_id=1, source_target_pairs={{0,1},{1,2},{2,3},{3,4},{4,5},{5,6},{6,7},{7,0},{8,9},{9,10},{10,1... | collective-permute-start | bytes 1572872 | tf_op jit(solution)/shard_map/ppermute | solution.py:16
  74.1 166.2 %reduce-scatter.2.cloned.1.call-start = ((), (), s32[]{:S(2)}) async-start(), calls=%async_computation.4 | async-start | bytes 9437184 | tf_op jit(solution)/shard_map/reduce_scatter | solution.py:30
Sparse Core Ops, SparseCore 0:
  9.2 44.2 all-gather.3
  55.3 41.5 all-gather.5
  98.7 41.5 all-gather.7
  150.8 89.5 reduce-scatter.1
